TPU v7x, 32 devices: a whole 2x2x4 slice. The times are simulated.
32 devices in a mesh: sp: 8 (over z, y), tp: 4 (over x, core).
Axes of the slice: x: 2, y: 2, z: 4, core: 2. Of those that a mesh axis runs over, the one named last changes fastest.
Arguments:
- residual_input_stream: bfloat16 [8192, 2048], P(('sp', 'tp')), may hold values from -6 to 6
- receptance: bfloat16 [8192, 1024], P('sp', 'tp'), may hold values from -6 to 6
- key_matrix_all: bfloat16 [8192, 1024], P('sp', 'tp'), may hold values from -6 to 6
- value_matrix_all: bfloat16 [8192, 1024], P('sp', 'tp'), may hold values from -6 to 6
- decay_preactivation: bfloat16 [8192, 1024], P('sp', 'tp'), may hold values from -15 to 1
- learning_rate_preactivation: bfloat16 [8192, 1024], P('sp', 'tp'), may hold values from -11 to 5
- output_gate_all_heads: bfloat16 [8192, 1024], P('sp', 'tp'), may hold values from -6 to 6
- extra_log_decay: float32 [8192, 1024], P('sp', 'tp'), may hold values from -0.7 to 0
- head_norm_gain: float32 [1024], P('tp'), may hold values from 0.1 to 1.9
- output_projection_weight: bfloat16 [1024, 2048], P('tp'), may hold values from -0.1875 to 0.1875
- feedforward_norm_gain: float32 [2048], replicated, may hold values from 0.1 to 1.9
- gate_projection_weight: bfloat16 [2048, 5632], P('sp', 'tp'), may hold values from -0.125 to 0.125
- up_projection_weight: bfloat16 [2048, 5632], P('sp', 'tp'), may hold values from -0.125 to 0.125
- down_projection_weight: bfloat16 [2048, 5632], P('sp', 'tp'), may hold values from -0.078125 to 0.078125
- convolution_kernel: bfloat16 [3, 2, 5632], P(None, None, 'tp'), may hold values from -3.5 to 3.5
Outputs:
- layer_out: bfloat16 [8192, 2048], P(('sp', 'tp'))
All inputs are finite; a program needn't handle non-finite values.
Results may differ from a plain program's by a relative error of at most 0.022.
Values may be sent and summed in bfloat16 or wider, within the bound.
A program may use at most 128 MiB of HBM per device.

v0:
```python
import functools

import jax
import jax.numpy as jnp
from jax import lax
from jax.experimental import pallas as pl
from jax.experimental.pallas import tpu as pltpu
from jax.sharding import PartitionSpec as P

HEAD_WIDTH = 64
BLOCK = 64
PER_STEP = 4
HALO = 16
LAG = 3
MESH = pl.DeviceIdType.MESH
WIDE = jnp.float32
NARROW = jnp.bfloat16


def mul(a, b, dims=((1,), (0,))):
    return lax.dot_general(
        a.astype(NARROW), b.astype(NARROW), (dims, ((), ())), preferred_element_type=WIDE
    )


def parts_of(a, count):
    found = []
    for _ in range(count):
        piece = a.astype(NARROW)
        found.append(piece)
        a = a - piece.astype(WIDE)
    return found


def fine_left(a, b, count, dims=((1,), (0,))):
    return sum(mul(piece, b, dims) for piece in parts_of(a, count))


def fine_right(a, b, count, dims=((1,), (0,))):
    return sum(mul(a, piece, dims) for piece in parts_of(b, count))


def head_mask(width):
    rows = lax.broadcasted_iota(jnp.int32, (width, width), 0) // HEAD_WIDTH
    lanes = lax.broadcasted_iota(jnp.int32, (width, width), 1) // HEAD_WIDTH
    return jnp.where(rows == lanes, 1.0, 0.0)


def stacked(a, mask):
    a = a.astype(NARROW)
    return jnp.concatenate([a] * (mask.shape[0] // a.shape[0]), axis=0) * mask


def fine_product(a, b, mask):
    a_high, a_low = parts_of(a, 2)
    b_high, b_low = (stacked(piece, mask) for piece in parts_of(b, 2))
    return mul(a_high, b_high) + mul(a_low, b_high) + mul(a_high, b_low)


def collapsed(a):
    heads = a.shape[0] // HEAD_WIDTH
    return sum(a[h * HEAD_WIDTH : (h + 1) * HEAD_WIDTH] for h in range(heads))


def recurrence(refs, local_ref, reach_ref, state, before_step):
    q_ref, k_ref, v_ref, decay_ref, rate_ref, extra_ref = refs
    tokens, width = q_ref.shape
    mask_wide = head_mask(width)
    mask = mask_wide.astype(NARROW)
    last = ((1,), (1,))
    first = ((0,), (0,))

    rows = lax.broadcasted_iota(jnp.int32, (width, width), 0)
    lanes = lax.broadcasted_iota(jnp.int32, (width, width), 1)
    state[:, :width] = jnp.zeros((width, width), WIDE)
    state[:, width:] = jnp.where(rows == lanes, 1.0, 0.0)

    def one(index, carry):
        before_step(index)
        token = lax.broadcasted_iota(jnp.int32, (BLOCK, width), 0)
        other = lax.broadcasted_iota(jnp.int32, (BLOCK, width), 1) % BLOCK
        strict = token > other
        within = token >= other
        eye = jnp.where(token == other, 1.0, 0.0)
        lower = jnp.where(
            lax.broadcasted_iota(jnp.int32, (BLOCK, BLOCK), 0)
            >= lax.broadcasted_iota(jnp.int32, (BLOCK, BLOCK), 1),
            1.0,
            0.0,
        ).astype(NARROW)
        ones = jnp.ones((BLOCK, width), NARROW)

        def window(part):
            return pl.ds(pl.multiple_of((index * PER_STEP + part) * BLOCK, BLOCK), BLOCK)

        prepared = []
        for part in range(PER_STEP):
            at = window(part)
            q = q_ref[at].astype(WIDE)
            k = k_ref[at].astype(WIDE)
            v = stacked(v_ref[at], mask)
            log_decay = (
                -jnp.exp(-0.5) * jax.nn.sigmoid(decay_ref[at].astype(WIDE)) + extra_ref[at]
            )
            rates = jax.nn.sigmoid(rate_ref[at].astype(WIDE))
            normed = k * lax.rsqrt(fine_left(k * k, mask, 2) + 1e-06)
            removal = normed * rates
            cum = fine_right(lower, log_decay, 3)
            previous = cum - log_decay
            middle = cum[BLOCK // 2 : BLOCK // 2 + 1]
            end = cum[BLOCK - 1 : BLOCK]
            back = jnp.exp(middle - cum)
            left = jnp.concatenate(
                [normed * jnp.exp(previous - middle), q * jnp.exp(cum - middle)], axis=0
            )
            by_key = mul(left, stacked(k * back, mask), last)
            by_removal = mul(left, stacked(removal * back, mask), last)
            key_rate = jnp.where(strict, by_key[:BLOCK], 0.0)
            removal_rate = jnp.where(strict, by_removal[:BLOCK], 0.0)
            key_out = jnp.where(within, by_key[BLOCK:], 0.0)
            removal_out = jnp.where(within, by_removal[BLOCK:], 0.0)
            inverse = eye
            size = 1
            while size < BLOCK:
                pair = (token // (2 * size) == other // (2 * size)) & (
                    token // size != other // size
                )
                piece = jnp.where(pair, removal_rate, 0.0)
                if size == 1:
                    inverse = inverse - piece
                else:
                    inverse = inverse - fine_product(
                        fine_product(inverse, piece, mask), inverse, mask
                    )
                size *= 2
            from_state = mul(inverse, stacked(normed * jnp.exp(previous), mask))
            keyed = mul(jnp.concatenate([key_rate, key_out], axis=0), v)
            offset = mul(inverse, stacked(keyed[:BLOCK], mask))
            reach = q * jnp.exp(cum) - mul(removal_out, stacked(from_state, mask))
            local = keyed[BLOCK:] - mul(removal_out, stacked(offset, mask))
            to_end = jnp.exp(end - cum)
            span = jnp.exp(fine_left(log_decay, ones, 3, first))
            prepared.append((from_state, offset, reach, local, k * to_end, removal * to_end, span))

        for part in range(PER_STEP):
            at = window(part)
            from_state, offset, reach, local, key_end, removal_end, span = prepared[part]
            now = state[...]
            both = mul(jnp.concatenate([from_state, reach], axis=0), now)
            correction = both[:BLOCK, :width] + offset
            local_ref[at] = local + both[BLOCK:, :width]
            reach_ref[at] = both[BLOCK:, width:]
            kept_value = mul(
                jnp.concatenate([key_end, -removal_end], axis=0),
                jnp.concatenate([v_ref[at].astype(WIDE), correction], axis=0),
                first,
            )
            kept_map = mul(-removal_end, both[:BLOCK, width:], first)
            state[:, :width] = now[:, :width] * span + kept_value * mask_wide
            state[:, width:] = now[:, width:] * span + kept_map * mask_wide
        return carry

    lax.fori_loop(0, tokens // (BLOCK * PER_STEP), one, 0)


def ring_plan(count):
    hops = count // 2

    def entries(weight, hop):
        if hop < hops - 1:
            return [(weight, 0, hop), (weight, 1, hop)]
        return [(weight, None, hop)]

    plan = []
    for weight in range(3):
        plan += entries(weight, 0)
    for hop in range(1, hops):
        plan += entries(0, hop) + entries(1, hop)
    for hop in range(1, hops):
        plan += entries(2, hop)
    return plan


class Ring:
    def __init__(self, axis, shards, gathered, sems):
        self.axis, self.shards, self.gathered, self.sems = axis, shards, gathered, sems
        self.count = lax.axis_size(axis)
        me = lax.axis_index(axis)
        odd = lax.rem(me, 2)
        self.place = (1 - odd) * (me // 2) + odd * (self.count - 1 - me // 2)
        self.plan = ring_plan(self.count)
        self.number = {}
        for at, (weight, half, hop) in enumerate(self.plan):
            for way in (0, 1):
                self.number[weight, way if half is None else half, hop, way] = at
        self.issued = 0
        self.waited = set()

    def index(self, offset):
        at = lax.rem(self.place + offset + 2 * self.count, self.count)
        upper = at // (self.count // 2)
        return (1 - upper) * 2 * at + upper * (2 * (self.count - 1 - at) + 1)

    def block(self, weight, half, offset):
        rows = self.shards[weight].shape[0]
        start = self.index(offset) * rows + half * (rows // 2)
        return self.gathered[weight].at[pl.ds(pl.multiple_of(start, rows // 2), rows // 2)]

    def copy(self, at, way):
        weight, half, hop = self.plan[at]
        half = way if half is None else half
        rows = self.shards[weight].shape[0] // 2
        back = -hop if way == 0 else hop
        target = self.block(weight, half, back)
        source = self.shards[weight].at[pl.ds(half * rows, rows)] if hop == 0 else target
        slot = 2 * at + way
        return pltpu.make_async_remote_copy(
            src_ref=source,
            dst_ref=target,
            send_sem=self.sems[0].at[slot],
            recv_sem=self.sems[1].at[slot],
            device_id={self.axis: self.index(1 if way == 0 else -1)},
            device_id_type=MESH,
        )

    def arrive(self, weight, half, hop, way):
        at = self.number[weight, half, hop, way]
        if (at, way) not in self.waited:
            self.waited.add((at, way))
            self.copy(at, way).wait_recv()

    def issue_to(self, target):
        while self.issued < min(target, len(self.plan)):
            weight, half, hop = self.plan[self.issued]
            for way in (0, 1):
                if hop > 0:
                    self.arrive(weight, way if half is None else half, hop - 1, way)
                self.copy(self.issued, way).start()
            self.issued += 1

    def issue_share(self, numerator, denominator):
        self.issue_to(len(self.plan) * numerator // denominator)

    def issue_through(self, weight, hop):
        while any(w == weight and h <= hop for w, _, h in self.plan[self.issued :]):
            self.issue_to(self.issued + 1)

    def arrive_hop(self, weight, hop, way):
        for half in (0, 1):
            if (weight, half, hop, way) in self.number:
                self.arrive(weight, half, hop, way)

    def arrive_all(self, weight):
        for hop in range(self.count // 2):
            for way in (0, 1):
                self.arrive_hop(weight, hop, way)

    def finish(self):
        for at in range(len(self.plan)):
            for way in (0, 1):
                self.copy(at, way).wait_send()


class Group:
    def __init__(self, axis):
        self.axis = axis
        self.count = lax.axis_size(axis)
        self.me = lax.axis_index(axis)
        self.half = self.count // 2

    def device(self, offset, sibling):
        side = lax.rem(self.me, 2)
        group = lax.rem(self.me // 2 + offset + self.half, self.half)
        return 2 * group + (1 - side if sibling else side)

    def copy(self, source, target, sems, slot, device):
        return pltpu.make_async_remote_copy(
            src_ref=source,
            dst_ref=target,
            send_sem=sems[0].at[slot],
            recv_sem=sems[1].at[slot],
            device_id={self.axis: device},
            device_id_type=MESH,
        )


class Spread:
    def __init__(self, group, source, block, side_sems, far_sems, pass_sems):
        self.group, self.source, self.block = group, source, block
        self.side_sems, self.far_sems, self.pass_sems = side_sems, far_sems, pass_sems
        self.others = range(1, group.half)

    def slot(self, piece, offset):
        return piece * (self.group.half - 1) + offset - 1

    def side(self, piece):
        group = self.group
        return group.copy(
            self.source(piece), self.block(group.me, piece), self.side_sems, piece,
            group.device(0, True),
        )

    def far(self, piece, offset):
        group = self.group
        return group.copy(
            self.source(piece), self.block(group.me, piece), self.far_sems,
            self.slot(piece, offset), group.device(offset, False),
        )

    def onward(self, piece, offset):
        group = self.group
        block = self.block(group.device(-offset, False), piece)
        return group.copy(
            block, block, self.pass_sems, self.slot(piece, offset), group.device(0, True)
        )

    def start(self, piece):
        for offset in self.others:
            self.far(piece, offset).start()
        self.side(piece).start()

    def hand_on(self, piece):
        for offset in self.others:
            self.far(piece, offset).wait_recv()
            self.onward(piece, offset).start()

    def arrive(self, piece):
        self.side(piece).wait_recv()
        for offset in self.others:
            self.onward(piece, offset).wait_recv()

    def finish(self, piece):
        self.side(piece).wait_send()
        for offset in self.others:
            self.far(piece, offset).wait_send()
            self.onward(piece, offset).wait_send()


def layer_kernel(
    q_in, k_in, v_in, decay_in, rate_in, extra_in, out_gate_in, residual_in, out_weight_in,
    gate_in, up_in, down_in, head_gain, ffn_gain, taps,
    out,
    q, k, v, decay, rate, extra, out_gate, local, reach, state, maps,
    stream, out_weight, mixed, normed, full_gate, full_up, full_down, hidden,
    part, near, leaving, far,
    load_sem, ring_send, ring_recv, map_send, map_recv, halo_send, halo_recv,
    rows_side_send, rows_side_recv, rows_far_send, rows_far_recv, rows_pass_send, rows_pass_recv,
    wide_side_send, wide_side_recv, wide_far_send, wide_far_recv, wide_pass_send, wide_pass_recv,
    mix_side_send, mix_side_recv, mix_far_send, mix_far_recv, mix_pass_send, mix_pass_recv,
    near_send, near_recv, far_send, far_recv,
):
    tokens, width = q.shape
    features = stream.shape[1]
    group = Group("tp")
    around = lax.axis_size("sp")
    place = lax.axis_index("sp")
    own_rows = tokens // group.count
    ring = Ring(
        "sp", (gate_in, up_in, down_in), (full_gate, full_up, full_down), (ring_send, ring_recv)
    )
    shard = down_in.shape[0]

    def owned(ref, index, rows):
        return ref.at[pl.ds(pl.multiple_of(index * rows, rows), rows)]

    pairs = list(
        zip(
            (q_in, k_in, v_in, decay_in, rate_in, extra_in, out_gate_in),
            (q, k, v, decay, rate, extra, out_gate),
        )
    )
    inputs = len(pairs)
    pairs += [
        (residual_in, owned(stream, group.me, own_rows)),
        (out_weight_in, owned(out_weight, group.me, width)),
        (gate_in, owned(full_gate, place, shard)),
        (up_in, owned(full_up, place, shard)),
        (down_in, owned(full_down, place, shard)),
    ]
    loads = [
        pltpu.make_async_copy(source, target, load_sem.at[at])
        for at, (source, target) in enumerate(pairs)
    ]
    for load in loads[:inputs]:
        load.start()

    barrier = pltpu.get_barrier_semaphore()
    for axis, count, me in (("sp", around, place), ("tp", group.count, group.me)):
        for step in range(1, count):
            pl.semaphore_signal(
                barrier, inc=1, device_id={axis: lax.rem(me + step, count)}, device_id_type=MESH
            )
    pl.semaphore_wait(barrier, around + group.count - 2)

    ring.issue_share(6, 21)
    rows_spread = Spread(
        group,
        lambda piece: residual_in,
        lambda index, piece: owned(stream, index, own_rows),
        (rows_side_send, rows_side_recv),
        (rows_far_send, rows_far_recv),
        (rows_pass_send, rows_pass_recv),
    )
    wide_spread = Spread(
        group,
        lambda piece: out_weight_in,
        lambda index, piece: owned(out_weight, index, width),
        (wide_side_send, wide_side_recv),
        (wide_far_send, wide_far_recv),
        (wide_pass_send, wide_pass_recv),
    )
    rows_spread.start(0)
    wide_spread.start(0)
    for load in loads[inputs:]:
        load.start()
    for load in loads[:inputs]:
        load.wait()

    def before_step(index):
        @pl.when(index == tokens // (BLOCK * PER_STEP) - 1)
        def _():
            ring.issue_share(8, 21)

    recurrence((q, k, v, decay, rate, extra), local, reach, state, before_step)

    def map_copy(step):
        return pltpu.make_async_remote_copy(
            src_ref=maps.at[place],
            dst_ref=maps.at[place],
            send_sem=map_send.at[step - 1],
            recv_sem=map_recv.at[step - 1],
            device_id={"sp": lax.rem(place + step, around)},
            device_id_type=MESH,
        )

    maps[place] = collapsed(state[...]).astype(NARROW)
    for step in range(1, around):
        map_copy(step).start()
    rows_spread.hand_on(0)
    wide_spread.hand_on(0)
    ring.issue_share(10, 21)
    for step in range(1, around):
        map_copy(step).wait_recv()

    mask = head_mask(width).astype(NARROW)

    def enter(step, entering):
        found = maps[step]
        high, low = parts_of(entering, 2)
        after = (
            found[:, :width].astype(WIDE)
            + mul(found[:, width:], stacked(high, mask))
            + mul(found[:, width:], stacked(low, mask))
        )
        return jnp.where(step < place, after, entering)

    entering = lax.fori_loop(0, around - 1, enter, jnp.zeros((HEAD_WIDTH, width), WIDE))
    state[:, :width] = stacked(entering, mask).astype(WIDE)

    pieces = group.count
    own_lanes = pl.ds(pl.multiple_of(group.me * width, width), width)

    def mixed_block(index, piece):
        rows = pl.ds(pl.multiple_of(piece * own_rows, own_rows), own_rows)
        return mixed.at[rows, pl.ds(pl.multiple_of(index * width, width), width)]

    mix_spread = Spread(
        group,
        lambda piece: mixed_block(group.me, piece),
        mixed_block,
        (mix_side_send, mix_side_recv),
        (mix_far_send, mix_far_recv),
        (mix_pass_send, mix_pass_recv),
    )

    def mix(piece, carry):
        rows = pl.ds(pl.multiple_of(piece * own_rows, own_rows), own_rows)
        readout = local[rows] + mul(reach[rows], state[:, :width])
        centered = readout - fine_left(readout, mask, 2) * (1.0 / HEAD_WIDTH)
        variance = fine_left(centered * centered, mask, 2) * (1.0 / HEAD_WIDTH)
        value = (
            centered
            * lax.rsqrt(variance + 0.00064)
            * head_gain[...]
            * out_gate[rows].astype(WIDE)
        )
        mixed[rows, own_lanes] = value.astype(NARROW)
        mix_spread.start(piece)
        return carry

    lax.fori_loop(0, pieces, mix, 0)
    ring.issue_share(12, 21)
    rows_spread.arrive(0)
    wide_spread.arrive(0)
    rows_spread.finish(0)
    wide_spread.finish(0)
    loads[inputs].wait()
    loads[inputs + 1].wait()

    def settle(piece, carry):
        @pl.when(piece < pieces)
        def _():
            mix_spread.hand_on(piece)

        @pl.when(piece > 0)
        def _():
            done = piece - 1
            mix_spread.arrive(done)
            rows = pl.ds(pl.multiple_of(done * own_rows, own_rows), own_rows)
            total = mul(mixed[rows], out_weight[...])
            kept = (stream[rows].astype(WIDE) + total).astype(NARROW)
            stream[rows] = kept
            kept = kept.astype(WIDE)
            scale = lax.rsqrt(jnp.mean(kept * kept, axis=-1, keepdims=True) + 1e-06)
            after = pl.ds(pl.multiple_of(HALO + done * own_rows, HALO), own_rows)
            normed[after] = (kept * scale * ffn_gain[...]).astype(NARROW)

        return carry

    lax.fori_loop(0, pieces + 1, settle, 0)

    halo = pltpu.make_async_remote_copy(
        src_ref=normed.at[pl.ds(tokens, HALO)],
        dst_ref=normed.at[pl.ds(0, HALO)],
        send_sem=halo_send,
        recv_sem=halo_recv,
        device_id={"sp": lax.rem(place + 1, around)},
        device_id_type=MESH,
    )

    @pl.when(place < around - 1)
    def _():
        halo.start()

    @pl.when(place == 0)
    def _():
        normed[:HALO] = jnp.zeros((HALO, features), NARROW)

    ring.issue_share(18, 21)

    @pl.when(place > 0)
    def _():
        halo.wait_recv()

    for weight in (0, 1):
        ring.arrive_all(weight)
        loads[inputs + 2 + weight].wait()

    def lift(piece, carry):
        start = pl.multiple_of(piece * own_rows, own_rows)
        rows = normed[pl.ds(start, own_rows + HALO)]
        mixes = []
        for way, weight in enumerate((full_gate, full_up)):
            held = mul(rows, weight[...]).astype(NARROW).astype(WIDE)
            tap = [taps[at][way : way + 1].astype(WIDE) for at in range(3)]
            mixes.append(
                tap[0] * held[HALO - 2 : -2] + tap[1] * held[HALO - 1 : -1] + tap[2] * held[HALO:]
            )
        hidden[pl.ds(start, own_rows)] = (jax.nn.silu(mixes[0]) * mixes[1]).astype(NARROW)

        @pl.when(piece == pieces // 2)
        def _():
            ring.issue_share(19, 21)

        return carry

    lax.fori_loop(0, pieces, lift, 0)
    ring.issue_share(20, 21)

    block = part.shape[2]
    blocks = part.shape[0]
    by_arrival = block == shard
    loads[inputs + 4].wait()
    if not by_arrival:
        ring.issue_to(len(ring.plan))
        ring.arrive_all(2)

    def lanes_of(at):
        if by_arrival:
            odd = lax.rem(at, 2)
            owner = ring.index((2 * odd - 1) * ((at + 1) // 2))
        else:
            owner = at
        return pl.ds(pl.multiple_of(owner * block, block), block)

    def quarter(device):
        return pl.ds(pl.multiple_of(device * own_rows, own_rows), own_rows)

    def near_copy(at, offset):
        return group.copy(
            part.at[at, quarter(group.device(offset, True))],
            near.at[at, offset],
            (near_send, near_recv),
            at * group.half + offset,
            group.device(0, True),
        )

    def far_copy(at, offset):
        return group.copy(
            leaving.at[at, offset - 1],
            far.at[at, offset - 1],
            (far_send, far_recv),
            at * (group.half - 1) + offset - 1,
            group.device(offset, False),
        )

    def close(at, carry):
        if by_arrival:
            for fixed in range(1, blocks):
                hop = (fixed + 1) // 2 - 1

                @pl.when(at == fixed)
                def _():
                    ring.issue_through(2, hop + 1)
                    if hop == around // 2 - 1:
                        ring.arrive_hop(2, hop, 0)
                        ring.arrive_hop(2, hop, 1)
                    else:
                        ring.arrive_hop(2, hop, way_of(fixed))

        @pl.when(at < blocks)
        def _():
            weight = full_down[lanes_of(at)]
            part[at] = mul(hidden[...], weight, ((1,), (1,))).astype(NARROW)
            for offset in list(range(1, group.half)) + [0]:
                near_copy(at, offset).start()

        @pl.when((at >= 1) & (at <= blocks))
        def _():
            done = at - 1
            for offset in range(1, group.half):
                near_copy(done, offset).wait_recv()
                mine = part[done, quarter(group.device(offset, False))].astype(WIDE)
                total = mine + near[done, offset].astype(WIDE)
                leaving[done, offset - 1] = total.astype(NARROW)
                far_copy(done, offset).start()

        @pl.when(at >= LAG)
        def _():
            done = at - LAG
            near_copy(done, 0).wait_recv()
            own = quarter(group.me)
            total = part[done, own].astype(WIDE) + near[done, 0].astype(WIDE)
            for offset in range(1, group.half):
                far_copy(done, offset).wait_recv()
                total = total + far[done, offset - 1].astype(WIDE)
            lanes = lanes_of(done)
            out[:, lanes] = (stream[own, lanes].astype(WIDE) + total).astype(NARROW)

        return carry

    lax.fori_loop(0, blocks + LAG, close, 0)

    ring.finish()
    for step in range(1, around):
        map_copy(step).wait_send()

    @pl.when(place < around - 1)
    def _():
        halo.wait_send()

    def drain_mix(piece, carry):
        mix_spread.finish(piece)
        return carry

    lax.fori_loop(0, pieces, drain_mix, 0)

    def drain_sums(at, carry):
        for offset in range(group.half):
            near_copy(at, offset).wait_send()
        for offset in range(1, group.half):
            far_copy(at, offset).wait_send()
        return carry

    lax.fori_loop(0, blocks, drain_sums, 0)


def way_of(fixed):
    return 1 if fixed % 2 else 0


def layer(*arrays):
    (
        q, k, v, decay, rate, extra, out_gate, residual, out_weight, gate, up, down,
        head_gain, ffn_gain, taps,
    ) = arrays
    tokens, width = q.shape
    own_rows, features = residual.shape
    units = gate.shape[1]
    around, across = lax.axis_size("sp"), lax.axis_size("tp")
    shard = down.shape[0]
    block = shard if shard % 128 == 0 else 256
    blocks = features // block
    half = across // 2
    others = half - 1
    entries = 2 * len(ring_plan(around))
    dma = pltpu.SemaphoreType.DMA

    def two(count):
        return [dma((count,)), dma((count,))]

    def vmem(*shape, dtype=NARROW):
        return pltpu.VMEM(shape, dtype)

    anywhere = pl.BlockSpec(memory_space=pl.ANY)
    near_by = pl.BlockSpec(memory_space=pltpu.VMEM)
    return pl.pallas_call(
        layer_kernel,
        in_specs=[anywhere] * 12 + [near_by] * 3,
        out_specs=near_by,
        out_shape=jax.ShapeDtypeStruct((own_rows, features), NARROW),
        scratch_shapes=[vmem(tokens, width)] * 5
        + [
            vmem(tokens, width, dtype=WIDE),
            vmem(tokens, width),
            vmem(tokens, width, dtype=WIDE),
            vmem(tokens, width, dtype=WIDE),
            vmem(width, 2 * width, dtype=WIDE),
            vmem(around, HEAD_WIDTH, 2 * width),
            vmem(tokens, features),
            vmem(across * width, features),
            vmem(tokens, across * width),
            vmem(HALO + tokens, features),
            vmem(features, units),
            vmem(features, units),
            vmem(features, units),
            vmem(tokens, units),
            vmem(blocks, tokens, block),
            vmem(blocks, half, own_rows, block),
            vmem(blocks, others, own_rows, block),
            vmem(blocks, others, own_rows, block),
            dma((12,)),
        ]
        + two(entries)
        + two(around - 1)
        + [dma, dma]
        + (two(1) + two(others) + two(others)) * 2
        + two(across) + two(across * others) + two(across * others)
        + two(blocks * half)
        + two(blocks * others),
        compiler_params=pltpu.CompilerParams(
            collective_id=1, has_side_effects=True, vmem_limit_bytes=67043328
        ),
        name="layer",
    )(
        q, k, v, decay, rate, extra, out_gate, residual, out_weight, gate, up, down,
        head_gain[None], ffn_gain[None], taps,
    )


def body(
    residual_input_stream,
    receptance,
    key_matrix_all,
    value_matrix_all,
    decay_preactivation,
    learning_rate_preactivation,
    output_gate_all_heads,
    extra_log_decay,
    head_norm_gain,
    output_projection_weight,
    feedforward_norm_gain,
    gate_projection_weight,
    up_projection_weight,
    down_projection_weight,
    convolution_kernel,
):
    return layer(
        receptance,
        key_matrix_all,
        value_matrix_all,
        decay_preactivation,
        learning_rate_preactivation,
        extra_log_decay,
        output_gate_all_heads,
        residual_input_stream,
        output_projection_weight,
        gate_projection_weight,
        up_projection_weight,
        down_projection_weight,
        head_norm_gain,
        feedforward_norm_gain,
        convolution_kernel,
    )


def solution(mesh):
    in_specs = (
        P(("sp", "tp"), None),
        P("sp", "tp"),
        P("sp", "tp"),
        P("sp", "tp"),
        P("sp", "tp"),
        P("sp", "tp"),
        P("sp", "tp"),
        P("sp", "tp"),
        P("tp"),
        P("tp", None),
        P(),
        P("sp", "tp"),
        P("sp", "tp"),
        P("sp", "tp"),
        P(None, None, "tp"),
    )
    out_specs = P(("sp", "tp"), None)
    return jax.shard_map(
        body, mesh=mesh, in_specs=in_specs, out_specs=out_specs, check_vma=False
    )
```

profile of v0, /device:TPU:0, one launch (start us, length us, event | category | flops | bytes accessed | tf_op | source)
XLA Modules:
  0.0 195.4 jit_solution(3203908808670490777)
XLA Ops:
  0.0 193.1 %layer.1 = bf16[256,2048]{1,0:T(8,128)(2,1)} custom-call(bf16[1024,256]{1,0:T(8,128)(2,1)} %q_in.1, bf16[1024,256]{1,0:T(8,128)(2,1)} %k_in.1, bf16[1024,256]{1,0:T(8,128)(2,1)} %v_in.1, bf16[1024,256]{1,0:T(8,128)(2,1)} %decay_in.1, bf16[1024,256]{1,0:T(8,128)(2,1)} %rate_in.1, f32[1024,256]{1,0:T(8,128)} %extra_in.1, bf16[1024,256]{1,0:T(8,128)(2,1)} %out_gate_in.1, ...), custom_call_target="tpu_custom_call" | custom-call | tf_op jit(solution)/shard_map/layer/pallas_call | solution.py:707
  193.1 2.3 %copy.17 = bf16[256,2048]{1,0:T(8,128)(2,1)} copy(bf16[256,2048]{1,0:T(8,128)(2,1)} %layer.1) | data formatting | bytes 2097152
where the time goes:
time: 196 us; the launch traced here: 195 us
  Pallas kernels  193 us (98%)
  local copies, waits for them, and re-layouts  2.3 us (1%)
    pallas_call x1, Pallas kernels, layer(): pl.pallas_call(layer_kernel, in_specs=[anywhere] * 12 + [near_by] * 3, ou...  193 us

commit v1 on v0

--- a/solution.py
+++ b/solution.py
@@ -12,6 +12,7 @@
 PER_STEP = 4
 HALO = 16
 LAG = 3
+LATER = 2
 MESH = pl.DeviceIdType.MESH
 WIDE = jnp.float32
 NARROW = jnp.bfloat16
@@ -163,115 +164,41 @@
     lax.fori_loop(0, tokens // (BLOCK * PER_STEP), one, 0)
 
 
-def ring_plan(count):
-    hops = count // 2
-
-    def entries(weight, hop):
-        if hop < hops - 1:
-            return [(weight, 0, hop), (weight, 1, hop)]
-        return [(weight, None, hop)]
-
-    plan = []
-    for weight in range(3):
-        plan += entries(weight, 0)
-    for hop in range(1, hops):
-        plan += entries(0, hop) + entries(1, hop)
-    for hop in range(1, hops):
-        plan += entries(2, hop)
-    return plan
-
-
-class Ring:
-    def __init__(self, axis, shards, gathered, sems):
-        self.axis, self.shards, self.gathered, self.sems = axis, shards, gathered, sems
-        self.count = lax.axis_size(axis)
+def halves_of(units):
+    window = -(-units // 256) * 128
+    return window, units - window
+
+
+class Lines:
+    def __init__(self, axis, shards, gathered, over_sems, across_sems):
+        self.axis, self.shards, self.gathered = axis, shards, gathered
+        self.over_sems, self.across_sems = over_sems, across_sems
         me = lax.axis_index(axis)
-        odd = lax.rem(me, 2)
-        self.place = (1 - odd) * (me // 2) + odd * (self.count - 1 - me // 2)
-        self.plan = ring_plan(self.count)
-        self.number = {}
-        for at, (weight, half, hop) in enumerate(self.plan):
-            for way in (0, 1):
-                self.number[weight, way if half is None else half, hop, way] = at
-        self.issued = 0
-        self.waited = set()
-
-    def index(self, offset):
-        at = lax.rem(self.place + offset + 2 * self.count, self.count)
-        upper = at // (self.count // 2)
-        return (1 - upper) * 2 * at + upper * (2 * (self.count - 1 - at) + 1)
-
-    def block(self, weight, half, offset):
-        rows = self.shards[weight].shape[0]
-        start = self.index(offset) * rows + half * (rows // 2)
-        return self.gathered[weight].at[pl.ds(pl.multiple_of(start, rows // 2), rows // 2)]
-
-    def copy(self, at, way):
-        weight, half, hop = self.plan[at]
-        half = way if half is None else half
-        rows = self.shards[weight].shape[0] // 2
-        back = -hop if way == 0 else hop
-        target = self.block(weight, half, back)
-        source = self.shards[weight].at[pl.ds(half * rows, rows)] if hop == 0 else target
-        slot = 2 * at + way
-        return pltpu.make_async_remote_copy(
-            src_ref=source,
-            dst_ref=target,
-            send_sem=self.sems[0].at[slot],
-            recv_sem=self.sems[1].at[slot],
-            device_id={self.axis: self.index(1 if way == 0 else -1)},
-            device_id_type=MESH,
-        )
-
-    def arrive(self, weight, half, hop, way):
-        at = self.number[weight, half, hop, way]
-        if (at, way) not in self.waited:
-            self.waited.add((at, way))
-            self.copy(at, way).wait_recv()
-
-    def issue_to(self, target):
-        while self.issued < min(target, len(self.plan)):
-            weight, half, hop = self.plan[self.issued]
-            for way in (0, 1):
-                if hop > 0:
-                    self.arrive(weight, way if half is None else half, hop - 1, way)
-                self.copy(self.issued, way).start()
-            self.issued += 1
-
-    def issue_share(self, numerator, denominator):
-        self.issue_to(len(self.plan) * numerator // denominator)
-
-    def issue_through(self, weight, hop):
-        while any(w == weight and h <= hop for w, _, h in self.plan[self.issued :]):
-            self.issue_to(self.issued + 1)
-
-    def arrive_hop(self, weight, hop, way):
-        for half in (0, 1):
-            if (weight, half, hop, way) in self.number:
-                self.arrive(weight, half, hop, way)
-
-    def arrive_all(self, weight):
-        for hop in range(self.count // 2):
-            for way in (0, 1):
-                self.arrive_hop(weight, hop, way)
-
-    def finish(self):
-        for at in range(len(self.plan)):
-            for way in (0, 1):
-                self.copy(at, way).wait_send()
-
-
-class Group:
-    def __init__(self, axis):
-        self.axis = axis
-        self.count = lax.axis_size(axis)
-        self.me = lax.axis_index(axis)
-        self.half = self.count // 2
-
-    def device(self, offset, sibling):
-        side = lax.rem(self.me, 2)
-        group = lax.rem(self.me // 2 + offset + self.half, self.half)
-        return 2 * group + (1 - side if sibling else side)
+        self.outer = lax.axis_size(axis) // 2
+        self.line = me // 2
+        self.side = lax.rem(me, 2)
+        self.pair = self.line + 1 - 2 * lax.rem(self.line, 2)
+        self.shard = shards[0].shape[0]
+        self.step = self.shard // 2
+        self.window, self.shift = halves_of(shards[0].shape[1])
+
+    def share(self, line):
+        return lax.rem(line + line // 2, 2)
+
+    def lanes(self, line):
+        return pl.ds(pl.multiple_of(self.share(line) * self.shift, 128), self.window)
+
+    def line_at(self, offset):
+        return lax.rem(self.line + offset + self.outer, self.outer)
+
+    def source(self, entry, line):
+        weight, half = divmod(entry, 2)
+        return self.shards[weight].at[pl.ds(half * self.step, self.step), self.lanes(line)]
+
+    def target(self, entry, line, side):
+        weight, half = divmod(entry, 2)
+        start = (line * 2 + side) * self.shard + half * self.step
+        return self.gathered[weight].at[pl.ds(pl.multiple_of(start, self.step), self.step)]
 
     def copy(self, source, target, sems, slot, device):
         return pltpu.make_async_remote_copy(
@@ -283,6 +210,77 @@
             device_id_type=MESH,
         )
 
+    def over(self, entry, offset):
+        line = self.line_at(offset)
+        return self.copy(
+            self.source(entry, line),
+            self.target(entry, self.line, self.side),
+            self.over_sems,
+            entry * (self.outer - 1) + offset - 1,
+            line * 2 + self.side,
+        )
+
+    def across(self, entry, offset):
+        target = self.target(entry, self.line_at(-offset), self.side)
+        return self.copy(
+            self.source(entry, self.line) if offset == 0 else target,
+            target,
+            self.across_sems,
+            entry * self.outer + offset,
+            self.line * 2 + 1 - self.side,
+        )
+
+    def send(self, entry):
+        for offset in range(1, self.outer):
+            self.over(entry, offset).start()
+
+    def own(self, entry):
+        self.across(entry, 0).start()
+
+    def pump(self, entry):
+        for offset in range(1, self.outer):
+            self.over(entry, offset).wait_recv()
+            self.across(entry, offset).start()
+
+    def arrive(self, entry):
+        for offset in range(self.outer):
+            self.across(entry, offset).wait_recv()
+
+    def finish(self):
+        for entry in range(6):
+            for offset in range(1, self.outer):
+                self.over(entry, offset).wait_send()
+            for offset in range(self.outer):
+                self.across(entry, offset).wait_send()
+
+
+class Group:
+    def __init__(self, axis):
+        self.axis = axis
+        self.count = lax.axis_size(axis)
+        self.me = lax.axis_index(axis)
+        self.half = self.count // 2
+
+    def device(self, offset, sibling):
+        side = lax.rem(self.me, 2)
+        group = lax.rem(self.me // 2 + offset + self.half, self.half)
+        return 2 * group + (1 - side if sibling else side)
+
+    def turn(self, step, ahead):
+        side = lax.rem(self.me, 2)
+        group = lax.rem(self.me // 2 + ahead + step // 2, self.half)
+        return 2 * group + lax.rem(side + step, 2)
+
+    def copy(self, source, target, sems, slot, device):
+        return pltpu.make_async_remote_copy(
+            src_ref=source,
+            dst_ref=target,
+            send_sem=sems[0].at[slot],
+            recv_sem=sems[1].at[slot],
+            device_id={self.axis: device},
+            device_id_type=MESH,
+        )
+
 
 class Spread:
     def __init__(self, group, source, block, side_sems, far_sems, pass_sems):
@@ -341,13 +339,16 @@
     gate_in, up_in, down_in, head_gain, ffn_gain, taps,
     out,
     q, k, v, decay, rate, extra, out_gate, local, reach, state, maps,
-    stream, out_weight, mixed, normed, full_gate, full_up, full_down, hidden,
-    part, near, leaving, far,
-    load_sem, ring_send, ring_recv, map_send, map_recv, halo_send, halo_recv,
+    stream, out_weight, mixed, normed, others_normed, full_gate, full_up, full_down, hidden,
+    part, near, leaving, far, kept_sum, lent, returned, result,
+    load_sem, out_sem, over_send, over_recv, across_send, across_recv,
+    map_over_send, map_over_recv, map_across_send, map_across_recv,
+    halo_send, halo_recv, lend_send, lend_recv,
     rows_side_send, rows_side_recv, rows_far_send, rows_far_recv, rows_pass_send, rows_pass_recv,
     wide_side_send, wide_side_recv, wide_far_send, wide_far_recv, wide_pass_send, wide_pass_recv,
     mix_side_send, mix_side_recv, mix_far_send, mix_far_recv, mix_pass_send, mix_pass_recv,
-    near_send, near_recv, far_send, far_recv,
+    norm_side_send, norm_side_recv, norm_far_send, norm_far_recv, norm_pass_send, norm_pass_recv,
+    near_send, near_recv, far_send, far_recv, return_send, return_recv,
 ):
     tokens, width = q.shape
     features = stream.shape[1]
@@ -355,13 +356,19 @@
     around = lax.axis_size("sp")
     place = lax.axis_index("sp")
     own_rows = tokens // group.count
-    ring = Ring(
-        "sp", (gate_in, up_in, down_in), (full_gate, full_up, full_down), (ring_send, ring_recv)
-    )
+    lines = Lines(
+        "sp", (gate_in, up_in, down_in), (full_gate, full_up, full_down),
+        (over_send, over_recv), (across_send, across_recv),
+    )
+    outer, line, side = lines.outer, lines.line, lines.side
+    partner = lines.pair * 2 + side
     shard = down_in.shape[0]
 
     def owned(ref, index, rows):
         return ref.at[pl.ds(pl.multiple_of(index * rows, rows), rows)]
+
+    def at_sp(source, target, sems, slot, device):
+        return lines.copy(source, target, sems, slot, device)
 
     pairs = list(
         zip(
@@ -373,9 +380,10 @@
     pairs += [
         (residual_in, owned(stream, group.me, own_rows)),
         (out_weight_in, owned(out_weight, group.me, width)),
-        (gate_in, owned(full_gate, place, shard)),
-        (up_in, owned(full_up, place, shard)),
-        (down_in, owned(full_down, place, shard)),
+    ]
+    pairs += [
+        (whole.at[:, lines.lanes(line)], owned(full, place, shard))
+        for whole, full in zip(lines.shards, lines.gathered)
     ]
     loads = [
         pltpu.make_async_copy(source, target, load_sem.at[at])
@@ -392,7 +400,10 @@
             )
     pl.semaphore_wait(barrier, around + group.count - 2)
 
-    ring.issue_share(6, 21)
+    lines.send(0)
+    lines.send(1)
+    for entry in range(4):
+        lines.own(entry)
     rows_spread = Spread(
         group,
         lambda piece: residual_in,
@@ -416,31 +427,59 @@
     for load in loads[:inputs]:
         load.wait()
 
+    steps = tokens // (BLOCK * PER_STEP)
+
     def before_step(index):
-        @pl.when(index == tokens // (BLOCK * PER_STEP) - 1)
-        def _():
-            ring.issue_share(8, 21)
+        @pl.when(index == steps // 2)
+        def _():
+            lines.pump(0)
+            lines.own(4)
+            lines.own(5)
+            lines.send(2)
+
+        @pl.when(index == steps - 1)
+        def _():
+            lines.pump(1)
 
     recurrence((q, k, v, decay, rate, extra), local, reach, state, before_step)
 
-    def map_copy(step):
-        return pltpu.make_async_remote_copy(
-            src_ref=maps.at[place],
-            dst_ref=maps.at[place],
-            send_sem=map_send.at[step - 1],
-            recv_sem=map_recv.at[step - 1],
-            device_id={"sp": lax.rem(place + step, around)},
-            device_id_type=MESH,
+    def map_over(offset):
+        return at_sp(
+            maps.at[place], maps.at[place], (map_over_send, map_over_recv), offset - 1,
+            lax.rem(line + offset, outer) * 2 + side,
+        )
+
+    def map_across(offset):
+        held = maps.at[lines.line_at(-offset) * 2 + side]
+        return at_sp(
+            held, held, (map_across_send, map_across_recv), offset, line * 2 + 1 - side
         )
 
     maps[place] = collapsed(state[...]).astype(NARROW)
-    for step in range(1, around):
-        map_copy(step).start()
+    for offset in range(1, outer):
+
+        @pl.when(line + offset < outer)
+        def _():
+            map_over(offset).start()
+
+    map_across(0).start()
+    lines.send(3)
     rows_spread.hand_on(0)
     wide_spread.hand_on(0)
-    ring.issue_share(10, 21)
-    for step in range(1, around):
-        map_copy(step).wait_recv()
+    for offset in range(1, outer):
+
+        @pl.when(line >= offset)
+        def _():
+            map_over(offset).wait_recv()
+            map_across(offset).start()
+
+    lines.pump(2)
+    map_across(0).wait_recv()
+    for offset in range(1, outer):
+
+        @pl.when(line >= offset)
+        def _():
+            map_across(offset).wait_recv()
 
     mask = head_mask(width).astype(NARROW)
 
@@ -452,17 +491,19 @@
             + mul(found[:, width:], stacked(high, mask))
             + mul(found[:, width:], stacked(low, mask))
         )
-        return jnp.where(step < place, after, entering)
-
-    entering = lax.fori_loop(0, around - 1, enter, jnp.zeros((HEAD_WIDTH, width), WIDE))
+        return after
+
+    entering = lax.fori_loop(0, place, enter, jnp.zeros((HEAD_WIDTH, width), WIDE))
     state[:, :width] = stacked(entering, mask).astype(WIDE)
 
     pieces = group.count
     own_lanes = pl.ds(pl.multiple_of(group.me * width, width), width)
 
+    def rows_at(piece):
+        return pl.ds(pl.multiple_of(piece * own_rows, own_rows), own_rows)
+
     def mixed_block(index, piece):
-        rows = pl.ds(pl.multiple_of(piece * own_rows, own_rows), own_rows)
-        return mixed.at[rows, pl.ds(pl.multiple_of(index * width, width), width)]
+        return mixed.at[rows_at(piece), pl.ds(pl.multiple_of(index * width, width), width)]
 
     mix_spread = Spread(
         group,
@@ -473,8 +514,9 @@
         (mix_pass_send, mix_pass_recv),
     )
 
-    def mix(piece, carry):
-        rows = pl.ds(pl.multiple_of(piece * own_rows, own_rows), own_rows)
+    def mix(step, carry):
+        piece = group.turn(step, 1)
+        rows = rows_at(piece)
         readout = local[rows] + mul(reach[rows], state[:, :width])
         centered = readout - fine_left(readout, mask, 2) * (1.0 / HEAD_WIDTH)
         variance = fine_left(centered * centered, mask, 2) * (1.0 / HEAD_WIDTH)
@@ -489,7 +531,7 @@
         return carry
 
     lax.fori_loop(0, pieces, mix, 0)
-    ring.issue_share(12, 21)
+    lines.send(4)
     rows_spread.arrive(0)
     wide_spread.arrive(0)
     rows_spread.finish(0)
@@ -497,16 +539,37 @@
     loads[inputs].wait()
     loads[inputs + 1].wait()
 
-    def settle(piece, carry):
-        @pl.when(piece < pieces)
-        def _():
-            mix_spread.hand_on(piece)
-
-        @pl.when(piece > 0)
-        def _():
-            done = piece - 1
+    small = own_rows // pieces
+
+    def lend_rows(index, piece):
+        start = HALO + index * own_rows + piece * small
+        return pl.ds(pl.multiple_of(start, HALO), small)
+
+    def lend(piece):
+        rows = lend_rows(group.me, piece)
+        return at_sp(
+            normed.at[rows], others_normed.at[rows], (lend_send, lend_recv), piece, partner
+        )
+
+    norm_spread = Spread(
+        group,
+        lambda piece: others_normed.at[lend_rows(group.me, piece)],
+        lambda index, piece: others_normed.at[lend_rows(index, piece)],
+        (norm_side_send, norm_side_recv),
+        (norm_far_send, norm_far_recv),
+        (norm_pass_send, norm_pass_recv),
+    )
+
+    def settle(step, carry):
+        @pl.when(step < pieces)
+        def _():
+            mix_spread.hand_on(group.turn(step, 0))
+
+        @pl.when(step > 0)
+        def _():
+            done = group.turn(step - 1, 0)
             mix_spread.arrive(done)
-            rows = pl.ds(pl.multiple_of(done * own_rows, own_rows), own_rows)
+            rows = rows_at(done)
             total = mul(mixed[rows], out_weight[...])
             kept = (stream[rows].astype(WIDE) + total).astype(NARROW)
             stream[rows] = kept
@@ -515,168 +578,270 @@
             after = pl.ds(pl.multiple_of(HALO + done * own_rows, HALO), own_rows)
             normed[after] = (kept * scale * ffn_gain[...]).astype(NARROW)
 
+        @pl.when(step == 1)
+        def _():
+            for piece in range(pieces):
+                lend(piece).start()
+
         return carry
 
     lax.fori_loop(0, pieces + 1, settle, 0)
 
-    halo = pltpu.make_async_remote_copy(
-        src_ref=normed.at[pl.ds(tokens, HALO)],
-        dst_ref=normed.at[pl.ds(0, HALO)],
-        send_sem=halo_send,
-        recv_sem=halo_recv,
-        device_id={"sp": lax.rem(place + 1, around)},
-        device_id_type=MESH,
+    following = place + 1
+    following_pair = (
+        following // 2 + 1 - 2 * lax.rem(following // 2, 2)
+    ) * 2 + lax.rem(following, 2)
+    tail, head = pl.ds(tokens, HALO), pl.ds(0, HALO)
+    halo_sems = (halo_send, halo_recv)
+    halo = at_sp(normed.at[tail], normed.at[head], halo_sems, 0, lax.rem(following, around))
+    halo_lent = at_sp(
+        normed.at[tail], others_normed.at[head], halo_sems, 1, lax.rem(following_pair, around)
     )
 
     @pl.when(place < around - 1)
     def _():
         halo.start()
+        halo_lent.start()
 
     @pl.when(place == 0)
     def _():
         normed[:HALO] = jnp.zeros((HALO, features), NARROW)
 
-    ring.issue_share(18, 21)
+    @pl.when(partner == 0)
+    def _():
+        others_normed[:HALO] = jnp.zeros((HALO, features), NARROW)
+
+    lines.send(5)
+    lines.pump(3)
 
     @pl.when(place > 0)
     def _():
         halo.wait_recv()
 
-    for weight in (0, 1):
-        ring.arrive_all(weight)
-        loads[inputs + 2 + weight].wait()
-
-    def lift(piece, carry):
+    for entry in range(4):
+        lines.arrive(entry)
+    loads[inputs + 2].wait()
+    loads[inputs + 3].wait()
+    spare = lines.window - lines.shift
+
+    def lift(source, base, piece):
         start = pl.multiple_of(piece * own_rows, own_rows)
-        rows = normed[pl.ds(start, own_rows + HALO)]
+        rows = source[pl.ds(start, own_rows + HALO)]
         mixes = []
         for way, weight in enumerate((full_gate, full_up)):
             held = mul(rows, weight[...]).astype(NARROW).astype(WIDE)
-            tap = [taps[at][way : way + 1].astype(WIDE) for at in range(3)]
+            tap = [taps[at, pl.ds(way, 1), lines.lanes(line)].astype(WIDE) for at in range(3)]
             mixes.append(
                 tap[0] * held[HALO - 2 : -2] + tap[1] * held[HALO - 1 : -1] + tap[2] * held[HALO:]
             )
-        hidden[pl.ds(start, own_rows)] = (jax.nn.silu(mixes[0]) * mixes[1]).astype(NARROW)
-
-        @pl.when(piece == pieces // 2)
-        def _():
-            ring.issue_share(19, 21)
-
+        to = pl.ds(pl.multiple_of(base + start, own_rows), own_rows)
+        hidden[to] = (jax.nn.silu(mixes[0]) * mixes[1]).astype(NARROW)
+        if spare:
+
+            @pl.when(lines.share(line) == 1)
+            def _():
+                hidden[to, :spare] = jnp.zeros((own_rows, spare), NARROW)
+
+    def lift_own(piece, carry):
+        lend(piece).wait_recv()
+        norm_spread.start(piece)
+
+        @pl.when(piece > 0)
+        def _():
+            norm_spread.hand_on(piece - 1)
+
+        lift(normed, 0, piece)
         return carry
 
-    lax.fori_loop(0, pieces, lift, 0)
-    ring.issue_share(20, 21)
+    lax.fori_loop(0, pieces, lift_own, 0)
+    norm_spread.hand_on(pieces - 1)
+    lines.pump(4)
 
     block = part.shape[2]
-    blocks = part.shape[0]
-    by_arrival = block == shard
+    slots = part.shape[0]
+    spans = slots // 2
+    units = 2 * slots
+    by_arrival = lines.step == block // 2 and spans == outer
+    lines.arrive(4)
     loads[inputs + 4].wait()
+
+    def last_weights():
+        lines.pump(5)
+        lines.arrive(5)
+
     if not by_arrival:
-        ring.issue_to(len(ring.plan))
-        ring.arrive_all(2)
-
-    def lanes_of(at):
+        last_weights()
+
+    def feature_block(unit):
+        return unit // (2 * spans) * spans + lax.rem(unit, spans)
+
+    def whose(unit):
+        return lax.rem(unit // spans, 2)
+
+    def starts_of(index):
         if by_arrival:
-            odd = lax.rem(at, 2)
-            owner = ring.index((2 * odd - 1) * ((at + 1) // 2))
+            first = lax.rem(index, spans) * 2 * shard + index // spans * lines.step
+            found = (first, first + shard)
         else:
-            owner = at
-        return pl.ds(pl.multiple_of(owner * block, block), block)
-
-    def quarter(device):
-        return pl.ds(pl.multiple_of(device * own_rows, own_rows), own_rows)
-
-    def near_copy(at, offset):
+            found = (index * block, index * block + block // 2)
+        return [pl.ds(pl.multiple_of(start, block // 2), block // 2) for start in found]
+
+    def near_copy(unit, offset):
         return group.copy(
-            part.at[at, quarter(group.device(offset, True))],
-            near.at[at, offset],
+            part.at[lax.rem(unit, slots), rows_at(group.device(offset, True))],
+            near.at[unit, offset],
             (near_send, near_recv),
-            at * group.half + offset,
+            unit * group.half + offset,
             group.device(0, True),
         )
 
-    def far_copy(at, offset):
+    def far_copy(unit, offset):
         return group.copy(
-            leaving.at[at, offset - 1],
-            far.at[at, offset - 1],
+            leaving.at[unit, offset - 1],
+            far.at[unit, offset - 1],
             (far_send, far_recv),
-            at * (group.half - 1) + offset - 1,
+            unit * (group.half - 1) + offset - 1,
             group.device(offset, False),
         )
 
-    def close(at, carry):
-        if by_arrival:
-            for fixed in range(1, blocks):
-                hop = (fixed + 1) // 2 - 1
-
-                @pl.when(at == fixed)
-                def _():
-                    ring.issue_through(2, hop + 1)
-                    if hop == around // 2 - 1:
-                        ring.arrive_hop(2, hop, 0)
-                        ring.arrive_hop(2, hop, 1)
-                    else:
-                        ring.arrive_hop(2, hop, way_of(fixed))
-
-        @pl.when(at < blocks)
-        def _():
-            weight = full_down[lanes_of(at)]
-            part[at] = mul(hidden[...], weight, ((1,), (1,))).astype(NARROW)
+    def give_back(index):
+        return at_sp(
+            lent.at[index], returned.at[index], (return_send, return_recv), index, partner
+        )
+
+    def out_copy(index, way):
+        lanes = starts_of(index)[way]
+        return pltpu.make_async_copy(
+            result.at[:, lanes], out.at[:, lanes], out_sem.at[2 * index + way]
+        )
+
+    own = rows_at(group.me)
+
+    def close(step, carry):
+        pause = spans
+        unit = jnp.where(step > pause, step - 1, step)
+
+        @pl.when((step == 2 * spans + 1) & by_arrival)
+        def _():
+            if by_arrival:
+                last_weights()
+
+        @pl.when((step != pause) & (unit < units))
+        def _():
+            @pl.when(unit >= slots)
+            def _():
+                for offset in range(group.half):
+                    near_copy(unit - slots, offset).wait_send()
+
+            weight = jnp.concatenate(
+                [full_down[rows] for rows in starts_of(feature_block(unit))], axis=0
+            )
+            rows = hidden[pl.ds(pl.multiple_of(whose(unit) * tokens, tokens), tokens)]
+            part[lax.rem(unit, slots)] = mul(rows, weight, ((1,), (1,))).astype(NARROW)
             for offset in list(range(1, group.half)) + [0]:
-                near_copy(at, offset).start()
-
-        @pl.when((at >= 1) & (at <= blocks))
-        def _():
-            done = at - 1
+                near_copy(unit, offset).start()
+
+        ready = jnp.where(step > pause, step - 2, step - 1)
+
+        @pl.when((step >= 1) & (step != pause + 1) & (ready < units))
+        def _():
             for offset in range(1, group.half):
-                near_copy(done, offset).wait_recv()
-                mine = part[done, quarter(group.device(offset, False))].astype(WIDE)
-                total = mine + near[done, offset].astype(WIDE)
-                leaving[done, offset - 1] = total.astype(NARROW)
-                far_copy(done, offset).start()
-
-        @pl.when(at >= LAG)
-        def _():
-            done = at - LAG
+                near_copy(ready, offset).wait_recv()
+                mine = part[lax.rem(ready, slots), rows_at(group.device(offset, False))]
+                total = mine.astype(WIDE) + near[ready, offset].astype(WIDE)
+                leaving[ready, offset - 1] = total.astype(NARROW)
+                far_copy(ready, offset).start()
+
+        @pl.when(step == pause)
+        def _():
+            @pl.when(partner > 0)
+            def _():
+                halo_lent.wait_recv()
+
+            def lift_lent(piece, carry):
+                lift(others_normed, tokens, piece)
+                return carry
+
+            for piece in range(pieces):
+                norm_spread.arrive(piece)
+            lax.fori_loop(0, pieces, lift_lent, 0)
+
+        done = step - 1 - LAG
+
+        @pl.when((done >= 0) & (done < units))
+        def _():
             near_copy(done, 0).wait_recv()
-            own = quarter(group.me)
-            total = part[done, own].astype(WIDE) + near[done, 0].astype(WIDE)
+            total = part[lax.rem(done, slots), own].astype(WIDE) + near[done, 0].astype(WIDE)
             for offset in range(1, group.half):
                 far_copy(done, offset).wait_recv()
                 total = total + far[done, offset - 1].astype(WIDE)
-            lanes = lanes_of(done)
-            out[:, lanes] = (stream[own, lanes].astype(WIDE) + total).astype(NARROW)
+            index = feature_block(done)
+
+            @pl.when(whose(done) == 0)
+            def _():
+                kept = [stream[own, lanes].astype(WIDE) for lanes in starts_of(index)]
+                kept_sum[index] = total + jnp.concatenate(kept, axis=1)
+
+            @pl.when(whose(done) == 1)
+            def _():
+                lent[index] = total.astype(NARROW)
+                give_back(index).start()
+
+        last = done - LATER
+
+        @pl.when((last >= 0) & (last < units) & (whose(jnp.maximum(last, 0)) == 1))
+        def _():
+            index = feature_block(last)
+            give_back(index).wait_recv()
+            total = (kept_sum[index] + returned[index].astype(WIDE)).astype(NARROW)
+            for way, lanes in enumerate(starts_of(index)):
+                result[:, lanes] = total[:, way * (block // 2) : (way + 1) * (block // 2)]
+                out_copy(index, way).start()
 
         return carry
 
-    lax.fori_loop(0, blocks + LAG, close, 0)
-
-    ring.finish()
-    for step in range(1, around):
-        map_copy(step).wait_send()
+    lax.fori_loop(0, units + 1 + LAG + LATER, close, 0)
+
+    lines.finish()
+    map_across(0).wait_send()
+    for offset in range(1, outer):
+
+        @pl.when(line + offset < outer)
+        def _():
+            map_over(offset).wait_send()
+
+        @pl.when(line >= offset)
+        def _():
+            map_across(offset).wait_send()
 
     @pl.when(place < around - 1)
     def _():
         halo.wait_send()
-
-    def drain_mix(piece, carry):
+        halo_lent.wait_send()
+
+    for piece in range(pieces):
         mix_spread.finish(piece)
+        norm_spread.finish(piece)
+        lend(piece).wait_send()
+
+    def drain(unit, carry):
+        @pl.when(unit >= units - slots)
+        def _():
+            for offset in range(group.half):
+                near_copy(unit, offset).wait_send()
+
+        for offset in range(1, group.half):
+            far_copy(unit, offset).wait_send()
+
+        @pl.when(unit < slots)
+        def _():
+            give_back(unit).wait_send()
+            for way in (0, 1):
+                out_copy(unit, way).wait()
+
         return carry
 
-    lax.fori_loop(0, pieces, drain_mix, 0)
-
-    def drain_sums(at, carry):
-        for offset in range(group.half):
-            near_copy(at, offset).wait_send()
-        for offset in range(1, group.half):
-            far_copy(at, offset).wait_send()
-        return carry
-
-    lax.fori_loop(0, blocks, drain_sums, 0)
-
-
-def way_of(fixed):
-    return 1 if fixed % 2 else 0
+    lax.fori_loop(0, units, drain, 0)
 
 
 def layer(*arrays):
@@ -686,14 +851,14 @@
     ) = arrays
     tokens, width = q.shape
     own_rows, features = residual.shape
-    units = gate.shape[1]
+    window, _ = halves_of(gate.shape[1])
     around, across = lax.axis_size("sp"), lax.axis_size("tp")
-    shard = down.shape[0]
-    block = shard if shard % 128 == 0 else 256
-    blocks = features // block
+    outer = around // 2
+    block = 256
+    slots = features // block
+    work = 2 * slots
     half = across // 2
     others = half - 1
-    entries = 2 * len(ring_plan(around))
     dma = pltpu.SemaphoreType.DMA
 
     def two(count):
@@ -707,7 +872,7 @@
     return pl.pallas_call(
         layer_kernel,
         in_specs=[anywhere] * 12 + [near_by] * 3,
-        out_specs=near_by,
+        out_specs=anywhere,
         out_shape=jax.ShapeDtypeStruct((own_rows, features), NARROW),
         scratch_shapes=[vmem(tokens, width)] * 5
         + [
@@ -721,23 +886,33 @@
             vmem(across * width, features),
             vmem(tokens, across * width),
             vmem(HALO + tokens, features),
-            vmem(features, units),
-            vmem(features, units),
-            vmem(features, units),
-            vmem(tokens, units),
-            vmem(blocks, tokens, block),
-            vmem(blocks, half, own_rows, block),
-            vmem(blocks, others, own_rows, block),
-            vmem(blocks, others, own_rows, block),
+            vmem(HALO + tokens, features),
+            vmem(features, window),
+            vmem(features, window),
+            vmem(features, window),
+            vmem(2 * tokens, window),
+            vmem(slots, tokens, block),
+            vmem(work, half, own_rows, block),
+            vmem(work, others, own_rows, block),
+            vmem(work, others, own_rows, block),
+            vmem(slots, own_rows, block, dtype=WIDE),
+            vmem(slots, own_rows, block),
+            vmem(slots, own_rows, block),
+            vmem(own_rows, features),
             dma((12,)),
+            dma((2 * slots,)),
         ]
-        + two(entries)
-        + two(around - 1)
-        + [dma, dma]
+        + two(6 * (outer - 1))
+        + two(6 * outer)
+        + two(outer - 1)
+        + two(outer)
+        + two(2)
+        + two(across)
         + (two(1) + two(others) + two(others)) * 2
-        + two(across) + two(across * others) + two(across * others)
-        + two(blocks * half)
-        + two(blocks * others),
+        + (two(across) + two(across * others) + two(across * others)) * 2
+        + two(work * half)
+        + two(work * others)
+        + two(slots),
         compiler_params=pltpu.CompilerParams(
             collective_id=1, has_side_effects=True, vmem_limit_bytes=67043328
         ),

time: 196 us -> 239 us (1.22)
  the two profiles are of different devices: /device:TPU:0 before, /device:TPU:18 now
where the time goes in v1:
time: 239 us
  Pallas kernels  237 us (99%)
    pallas_call x1, Pallas kernels, layer(): pl.pallas_call(layer_kernel, in_specs=[anywhere] * 12 + [near_by] * 3, ou...  237 us

profile of v1, /device:TPU:18, one launch (start us, length us, event | category | flops | bytes accessed | tf_op | source)
XLA Modules:
  0.0 239.2 jit_solution(9443694285579859641)
XLA Ops:
  0.0 236.9 %layer.1 = bf16[256,2048]{1,0:T(8,128)(2,1)} custom-call(bf16[1024,256]{1,0:T(8,128)(2,1)} %q_in.1, bf16[1024,256]{1,0:T(8,128)(2,1)} %k_in.1, bf16[1024,256]{1,0:T(8,128)(2,1)} %v_in.1, bf16[1024,256]{1,0:T(8,128)(2,1)} %decay_in.1, bf16[1024,256]{1,0:T(8,128)(2,1)} %rate_in.1, f32[1024,256]{1,0:T(8,128)} %extra_in.1, bf16[1024,256]{1,0:T(8,128)(2,1)} %out_gate_in.1, ...), custom_call_target="tpu_custom_call" | custom-call | tf_op jit(solution)/shard_map/layer/pallas_call | solution.py:872
  236.9 2.3 copy.17

commit v2 on v0

--- a/solution.py
+++ b/solution.py
@@ -340,10 +340,11 @@
     q_in, k_in, v_in, decay_in, rate_in, extra_in, out_gate_in, residual_in, out_weight_in,
     gate_in, up_in, down_in, head_gain, ffn_gain, taps,
     out,
-    q, k, v, decay, rate, extra, out_gate, local, reach, state, maps,
+    q, k, v, decay, rate, extra, out_gate, local, reach, state, maps, passed,
     stream, out_weight, mixed, normed, full_gate, full_up, full_down, hidden,
-    part, near, leaving, far,
-    load_sem, ring_send, ring_recv, map_send, map_recv, halo_send, halo_recv,
+    part, near, leaving, far, result,
+    load_sem, out_sem, ring_send, ring_recv, map_over_send, map_over_recv,
+    map_across_send, map_across_recv, state_send, state_recv, halo_send, halo_recv,
     rows_side_send, rows_side_recv, rows_far_send, rows_far_recv, rows_pass_send, rows_pass_recv,
     wide_side_send, wide_side_recv, wide_far_send, wide_far_recv, wide_pass_send, wide_pass_recv,
     mix_side_send, mix_side_recv, mix_far_send, mix_far_recv, mix_pass_send, mix_pass_recv,
@@ -423,24 +424,71 @@
 
     recurrence((q, k, v, decay, rate, extra), local, reach, state, before_step)
 
-    def map_copy(step):
+    outer, line, side = around // 2, place // 2, lax.rem(place, 2)
+
+    def map_copy(index, sems, slot, device):
         return pltpu.make_async_remote_copy(
-            src_ref=maps.at[place],
-            dst_ref=maps.at[place],
-            send_sem=map_send.at[step - 1],
-            recv_sem=map_recv.at[step - 1],
-            device_id={"sp": lax.rem(place + step, around)},
+            src_ref=maps.at[index],
+            dst_ref=maps.at[index],
+            send_sem=sems[0].at[slot],
+            recv_sem=sems[1].at[slot],
+            device_id={"sp": device},
             device_id_type=MESH,
         )
 
+    def map_over(offset):
+        target = lax.rem(line + offset, outer) * 2 + side
+        return map_copy(place, (map_over_send, map_over_recv), offset - 1, target)
+
+    def map_across(offset):
+        held = lax.rem(line - offset + outer, outer) * 2 + side
+        return map_copy(
+            held, (map_across_send, map_across_recv), offset, line * 2 + 1 - side
+        )
+
+    states_on = pltpu.make_async_remote_copy(
+        src_ref=passed.at[1],
+        dst_ref=passed.at[0],
+        send_sem=state_send,
+        recv_sem=state_recv,
+        device_id={"sp": lax.rem(line + 1, outer) * 2 + side},
+        device_id_type=MESH,
+    )
+    last_line = line == outer - 1
+    before_last = line == outer - 2
+
     maps[place] = collapsed(state[...]).astype(NARROW)
-    for step in range(1, around):
-        map_copy(step).start()
+    for offset in range(1, outer):
+
+        @pl.when(line + offset < outer - 1)
+        def _():
+            map_over(offset).start()
+
+    @pl.when((side == 0) | before_last)
+    def _():
+        map_across(0).start()
+
     rows_spread.hand_on(0)
     wide_spread.hand_on(0)
-    ring.issue_share(10, 21)
-    for step in range(1, around):
-        map_copy(step).wait_recv()
+    ring.issue_share(9, 21)
+    for offset in range(1, outer):
+
+        @pl.when((line >= offset) & (line < outer - 1))
+        def _():
+            map_over(offset).wait_recv()
+            map_across(offset).start()
+
+    ring.issue_share(11, 21)
+
+    @pl.when((side == 1) | before_last)
+    def _():
+        map_across(0).wait_recv()
+
+    for offset in range(1, outer):
+
+        @pl.when((line >= offset) & (line < outer - 1))
+        def _():
+            map_across(offset).wait_recv()
 
     mask = head_mask(width).astype(NARROW)
 
@@ -452,10 +500,25 @@
             + mul(found[:, width:], stacked(high, mask))
             + mul(found[:, width:], stacked(low, mask))
         )
-        return jnp.where(step < place, after, entering)
-
-    entering = lax.fori_loop(0, around - 1, enter, jnp.zeros((HEAD_WIDTH, width), WIDE))
-    state[:, :width] = stacked(entering, mask).astype(WIDE)
+        return after
+
+    @pl.when(line < outer - 1)
+    def _():
+        passed[0] = lax.fori_loop(0, place, enter, jnp.zeros((HEAD_WIDTH, width), WIDE))
+
+    @pl.when(before_last)
+    def _():
+        passed[1] = lax.fori_loop(place, 2 * outer - 2, enter, passed[0])
+        states_on.start()
+
+    ring.issue_share(12, 21)
+
+    @pl.when(last_line)
+    def _():
+        states_on.wait_recv()
+        passed[0] = lax.fori_loop(2 * line, place, enter, passed[0])
+
+    state[:, :width] = stacked(passed[0], mask).astype(WIDE)
 
     pieces = group.count
     own_lanes = pl.ds(pl.multiple_of(group.me * width, width), width)
@@ -489,7 +552,7 @@
         return carry
 
     lax.fori_loop(0, pieces, mix, 0)
-    ring.issue_share(12, 21)
+    ring.issue_share(13, 21)
     rows_spread.arrive(0)
     wide_spread.arrive(0)
     rows_spread.finish(0)
@@ -604,7 +667,53 @@
             group.device(offset, False),
         )
 
+    def out_copy(at):
+        lanes = lanes_of(at)
+        return pltpu.make_async_copy(result.at[:, lanes], out.at[:, lanes], out_sem.at[at])
+
+    for offset in range(1, outer):
+
+        @pl.when(line + offset < outer - 1)
+        def _():
+            map_over(offset).wait_send()
+
+        @pl.when((line >= offset) & (line < outer - 1))
+        def _():
+            map_across(offset).wait_send()
+
+    @pl.when((side == 0) | before_last)
+    def _():
+        map_across(0).wait_send()
+
+    @pl.when(before_last)
+    def _():
+        states_on.wait_send()
+
+    @pl.when(place < around - 1)
+    def _():
+        halo.wait_send()
+
+    def drain(piece, carry):
+        mix_spread.finish(piece)
+        return carry
+
+    lax.fori_loop(0, pieces, drain, 0)
+
+    early = blocks - 3 if by_arrival else blocks
+
+    def pass_on(done):
+        for offset in range(1, group.half):
+            near_copy(done, offset).wait_recv()
+            mine = part[done, quarter(group.device(offset, False))].astype(WIDE)
+            total = mine + near[done, offset].astype(WIDE)
+            leaving[done, offset - 1] = total.astype(NARROW)
+            far_copy(done, offset).start()
+
     def close(at, carry):
+        @pl.when((at >= early) & (at <= blocks))
+        def _():
+            pass_on(at - 1)
+
         if by_arrival:
             for fixed in range(1, blocks):
                 hop = (fixed + 1) // 2 - 1
@@ -625,15 +734,9 @@
             for offset in list(range(1, group.half)) + [0]:
                 near_copy(at, offset).start()
 
-        @pl.when((at >= 1) & (at <= blocks))
-        def _():
-            done = at - 1
-            for offset in range(1, group.half):
-                near_copy(done, offset).wait_recv()
-                mine = part[done, quarter(group.device(offset, False))].astype(WIDE)
-                total = mine + near[done, offset].astype(WIDE)
-                leaving[done, offset - 1] = total.astype(NARROW)
-                far_copy(done, offset).start()
+        @pl.when((at >= 1) & (at < early))
+        def _():
+            pass_on(at - 1)
 
         @pl.when(at >= LAG)
         def _():
@@ -645,34 +748,24 @@
                 far_copy(done, offset).wait_recv()
                 total = total + far[done, offset - 1].astype(WIDE)
             lanes = lanes_of(done)
-            out[:, lanes] = (stream[own, lanes].astype(WIDE) + total).astype(NARROW)
+            result[:, lanes] = (stream[own, lanes].astype(WIDE) + total).astype(NARROW)
+            out_copy(done).start()
+            for offset in range(group.half):
+                near_copy(done, offset).wait_send()
+            for offset in range(1, group.half):
+                far_copy(done, offset).wait_send()
 
         return carry
 
     lax.fori_loop(0, blocks + LAG, close, 0)
 
     ring.finish()
-    for step in range(1, around):
-        map_copy(step).wait_send()
-
-    @pl.when(place < around - 1)
-    def _():
-        halo.wait_send()
-
-    def drain_mix(piece, carry):
-        mix_spread.finish(piece)
+
+    def flush(at, carry):
+        out_copy(at).wait()
         return carry
 
-    lax.fori_loop(0, pieces, drain_mix, 0)
-
-    def drain_sums(at, carry):
-        for offset in range(group.half):
-            near_copy(at, offset).wait_send()
-        for offset in range(1, group.half):
-            far_copy(at, offset).wait_send()
-        return carry
-
-    lax.fori_loop(0, blocks, drain_sums, 0)
+    lax.fori_loop(0, blocks, flush, 0)
 
 
 def way_of(fixed):
@@ -707,7 +800,7 @@
     return pl.pallas_call(
         layer_kernel,
         in_specs=[anywhere] * 12 + [near_by] * 3,
-        out_specs=near_by,
+        out_specs=anywhere,
         out_shape=jax.ShapeDtypeStruct((own_rows, features), NARROW),
         scratch_shapes=[vmem(tokens, width)] * 5
         + [
@@ -717,6 +810,7 @@
             vmem(tokens, width, dtype=WIDE),
             vmem(width, 2 * width, dtype=WIDE),
             vmem(around, HEAD_WIDTH, 2 * width),
+            vmem(2, HEAD_WIDTH, width, dtype=WIDE),
             vmem(tokens, features),
             vmem(across * width, features),
             vmem(tokens, across * width),
@@ -729,11 +823,14 @@
             vmem(blocks, half, own_rows, block),
             vmem(blocks, others, own_rows, block),
             vmem(blocks, others, own_rows, block),
+            vmem(own_rows, features),
             dma((12,)),
+            dma((blocks,)),
         ]
         + two(entries)
-        + two(around - 1)
-        + [dma, dma]
+        + two(around // 2 - 1)
+        + two(around // 2)
+        + [dma] * 4
         + (two(1) + two(others) + two(others)) * 2
         + two(across) + two(across * others) + two(across * others)
         + two(blocks * half)

time: 196 us -> 184 us (0.939)
  Pallas kernels: 193 us -> 181 us
    pallas_call x1, Pallas kernels: 193 us -> 181 us  [layer(): pl.pallas_call(layer_kernel, in_specs=[anywhere] * 12 + [near_by] * 3, ou...]
where the time goes in v2:
time: 184 us; the launch traced here: 183 us
  Pallas kernels  181 us (98%)
  local copies, waits for them, and re-layouts  2.3 us (1%)
    pallas_call x1, Pallas kernels, layer(): pl.pallas_call(layer_kernel, in_specs=[anywhere] * 12 + [near_by] * 3, ou...  181 us

profile of v2, /device:TPU:0, one launch (start us, length us, event | category | flops | bytes accessed | tf_op | source)
XLA Modules:
  0.0 183.0 jit_solution(5319690825557741926)
XLA Ops:
  0.0 180.7 %layer.1 = bf16[256,2048]{1,0:T(8,128)(2,1)} custom-call(bf16[1024,256]{1,0:T(8,128)(2,1)} %q_in.1, bf16[1024,256]{1,0:T(8,128)(2,1)} %k_in.1, bf16[1024,256]{1,0:T(8,128)(2,1)} %v_in.1, bf16[1024,256]{1,0:T(8,128)(2,1)} %decay_in.1, bf16[1024,256]{1,0:T(8,128)(2,1)} %rate_in.1, f32[1024,256]{1,0:T(8,128)} %extra_in.1, bf16[1024,256]{1,0:T(8,128)(2,1)} %out_gate_in.1, ...), custom_call_target="tpu_custom_call" | custom-call | tf_op jit(solution)/shard_map/layer/pallas_call | solution.py:800
  180.7 2.3 %copy.17 = bf16[256,2048]{1,0:T(8,128)(2,1)} copy(bf16[256,2048]{1,0:T(8,128)(2,1)} %layer.1) | data formatting | bytes 2097152

commit v3 on v2

--- a/solution.py
+++ b/solution.py
@@ -730,8 +730,11 @@
         @pl.when(at < blocks)
         def _():
             weight = full_down[lanes_of(at)]
-            part[at] = mul(hidden[...], weight, ((1,), (1,))).astype(NARROW)
+            both = 2 * own_rows
             for offset in list(range(1, group.half)) + [0]:
+                chip = group.device(offset, False) // 2
+                rows = pl.ds(pl.multiple_of(chip * both, both), both)
+                part[at, rows] = mul(hidden[rows], weight, ((1,), (1,))).astype(NARROW)
                 near_copy(at, offset).start()
 
         @pl.when((at >= 1) & (at < early))

time: 184 us -> 186 us (1.011)
  Pallas kernels: 181 us -> 184 us
    pallas_call x1, Pallas kernels: 181 us -> 184 us  [layer(): pl.pallas_call(layer_kernel, in_specs=[anywhere] * 12 + [near_by] * 3, ou...]
where the time goes in v3:
time: 186 us
  Pallas kernels  184 us (99%)
  local copies, waits for them, and re-layouts  2.3 us (1%)
    pallas_call x1, Pallas kernels, layer(): pl.pallas_call(layer_kernel, in_specs=[anywhere] * 12 + [near_by] * 3, ou...  184 us

profile of v3, /device:TPU:0, one launch (start us, length us, event | category | flops | bytes accessed | tf_op | source)
XLA Modules:
  0.0 185.9 jit_solution(7790179867716486691)
XLA Ops:
  0.0 183.6 %layer.1 = bf16[256,2048]{1,0:T(8,128)(2,1)} custom-call(bf16[1024,256]{1,0:T(8,128)(2,1)} %q_in.1, bf16[1024,256]{1,0:T(8,128)(2,1)} %k_in.1, bf16[1024,256]{1,0:T(8,128)(2,1)} %v_in.1, bf16[1024,256]{1,0:T(8,128)(2,1)} %decay_in.1, bf16[1024,256]{1,0:T(8,128)(2,1)} %rate_in.1, f32[1024,256]{1,0:T(8,128)} %extra_in.1, bf16[1024,256]{1,0:T(8,128)(2,1)} %out_gate_in.1, ...), custom_call_target="tpu_custom_call" | custom-call | tf_op jit(solution)/shard_map/layer/pallas_call | solution.py:803
  183.6 2.3 %copy.17 = bf16[256,2048]{1,0:T(8,128)(2,1)} copy(bf16[256,2048]{1,0:T(8,128)(2,1)} %layer.1) | data formatting | bytes 2097152
